TPU v7x, 32 devices: a whole 2x2x4 slice. The times are simulated.
32 devices in a mesh: grp: 2 (over y), sp: 4 (over z), tp: 4 (over x, core).
Axes of the slice: x: 2, y: 2, z: 4, core: 2. Of those that a mesh axis runs over, the one named last changes fastest.
Arguments:
- latent: bfloat16 [2048, 512], P(('grp', 'sp')), parts along dimension 0, may hold values from -6 to 6
- rope_key: bfloat16 [2048, 64], P(('grp', 'sp')), parts along dimension 0, may hold values from -6 to 6
- wide_query: bfloat16 [2048, 1536], P(('grp', 'sp'), 'tp'), parts along dimension 0, may hold values from -1300 to 1300
- narrow_query: bfloat16 [2048, 1024], P(('grp', 'sp'), 'tp'), parts along dimension 0, may hold values from -1300 to 1300
- wide_key_weight: bfloat16 [512, 1024], P(None, 'tp'), may hold values from -0.25 to 0.25
- wide_value_weight: bfloat16 [512, 1024], P(None, 'tp'), may hold values from -0.25 to 0.25
- narrow_key_weight: bfloat16 [512, 512], P(None, 'tp'), may hold values from -0.25 to 0.25
- narrow_value_weight: bfloat16 [512, 512], P(None, 'tp'), may hold values from -0.25 to 0.25
- latent_norm_scale: float32 [512], replicated, may hold values from 0.1 to 1.9
- out_wide: bfloat16 [1024, 4096], P('tp'), may hold values from -0.4375 to 0.4375
- out_narrow: bfloat16 [512, 4096], P('tp'), may hold values from -0.4375 to 0.4375
- residual: bfloat16 [2048, 4096], P(('grp', 'sp', 'tp')), parts along dimension 0, may hold values from -6 to 6
- ffn_gain: float32 [4096], replicated, may hold values from 0.1 to 1.9
- shared_gate: bfloat16 [4096, 512], P(None, 'tp'), may hold values from -0.09375 to 0.09375
- shared_up: bfloat16 [4096, 512], P(None, 'tp'), may hold values from -0.09375 to 0.09375
- shared_down: bfloat16 [512, 4096], P('tp'), may hold values from -0.25 to 0.25
- expert_gate: bfloat16 [16, 4096, 192], P(('sp', 'tp')), may hold values from -0.09375 to 0.09375
- expert_up: bfloat16 [16, 4096, 192], P(('sp', 'tp')), may hold values from -0.09375 to 0.09375
- expert_down: bfloat16 [16, 192, 4096], P(('sp', 'tp')), may hold values from -0.4375 to 0.4375
- routes: int32 [2048, 2], P(('grp', 'sp', 'tp')), parts along dimension 0, may hold values from 0 to 15, all different within a row; in each aligned block of 64 rows (0 to 63, 64 to 127, ...) at most 16 rows name the same one
- route_weights: float32 [2048, 2], P(('grp', 'sp', 'tp')), parts along dimension 0, may hold values from 0.25 to 1.5
Outputs:
- layer_out: bfloat16 [2048, 4096], P(('grp', 'sp', 'tp')), parts along dimension 0
There are 2 independent parts, one for each index of `grp`. A program takes and returns all parts, laid end to end along the dimension named above; an argument that names none is the same for every part. Nothing has to cross between parts.
Inputs may be any that keep to these rules, and one draw needn't show every extreme that they name: `routes`: each row names 2 different experts; in each aligned block of 64 rows no expert is named by more than 16 rows, and some block has an expert named exactly 16 times.
All inputs are finite; a program needn't handle non-finite values.
Results may differ from a plain program's by a relative error of at most 0.023.
Values may be sent and summed in bfloat16 or wider, within the bound.
A program may use at most 128 MiB of HBM per device.

v0:
```python
import math
import jax
import jax.numpy as jnp
from jax import lax
from jax.sharding import PartitionSpec as P

ROPE = 64
WIDE_HEAD_SIZE = 128
NARROW_HEAD_SIZE = 64
EPS = 1e-06
ROPE_BASE = 10000.0
NEG_FILL = -1e30


def rotate(values, positions):
    half_size = values.shape[-1] // 2
    inverse = ROPE_BASE ** (-jnp.arange(half_size, dtype=jnp.float32) * 2.0 / values.shape[-1])
    angles = positions.astype(jnp.float32)[:, None] * inverse[None, :]
    shaped = (angles.shape[0],) + (1,) * (values.ndim - 2) + (half_size,)
    cosine_table = jnp.cos(angles).reshape(shaped)
    sine_table = jnp.sin(angles).reshape(shaped)
    first_half = values[..., :half_size]
    second_half = values[..., half_size:]
    return jnp.concatenate(
        [
            first_half * cosine_table - second_half * sine_table,
            second_half * cosine_table + first_half * sine_table,
        ],
        axis=-1,
    )


def rms_scale(values, gain):
    return values * lax.rsqrt(jnp.mean(values * values, axis=-1, keepdims=True) + EPS) * gain


def update(state, query_plain, query_turned, keys, turned_rows, values, visible, factor):
    running_max, running_sum, weighted = state
    scores = jnp.einsum("qhd,khd->hqk", query_plain, keys, preferred_element_type=jnp.float32)
    scores = scores + jnp.einsum(
        "qhr,kr->hqk", query_turned, turned_rows, preferred_element_type=jnp.float32
    )
    scores = jnp.where(visible[None], scores * factor, NEG_FILL)
    new_max = jnp.maximum(running_max, jnp.max(scores, axis=2))
    probs = jnp.where(visible[None], jnp.exp(scores - new_max[:, :, None]), 0.0)
    fading = jnp.exp(running_max - new_max)
    running_sum = running_sum * fading + jnp.sum(probs, axis=2)
    weighted = weighted * fading[:, :, None] + jnp.einsum(
        "hqk,khd->hqd", probs.astype(jnp.bfloat16), values, preferred_element_type=jnp.float32
    )
    return (new_max, running_sum, weighted)


def empty_state(heads, queries, value_size):
    return (
        jnp.full((heads, queries), NEG_FILL, jnp.float32),
        jnp.zeros((heads, queries), jnp.float32),
        jnp.zeros((heads, queries, value_size), jnp.float32),
    )


def finish(state):
    normal_sampler = state[2] / state[1][:, :, None]
    heads, queries, value_size = normal_sampler.shape
    return (
        normal_sampler.astype(jnp.bfloat16).transpose(1, 0, 2).reshape(queries, heads * value_size)
    )


def body(
    latent,
    rope_key,
    wide_query,
    narrow_query,
    wide_key_weight,
    wide_value_weight,
    narrow_key_weight,
    narrow_value_weight,
    latent_norm_scale,
    out_wide,
    out_narrow,
    residual,
    ffn_gain,
    shared_gate,
    shared_up,
    shared_down,
    expert_gate,
    expert_up,
    expert_down,
    routes,
    route_weights,
):
    tok_dev = latent.shape[0]
    seq_index = lax.axis_index("sp")
    own_pos = seq_index * tok_dev + jnp.arange(tok_dev, dtype=jnp.int32)
    last_pos = seq_index * tok_dev + tok_dev - 1
    normed_latent = rms_scale(latent.astype(jnp.float32), latent_norm_scale).astype(jnp.bfloat16)
    turned_key = rotate(rope_key.astype(jnp.float32), own_pos).astype(jnp.bfloat16)
    wide_heads_q = wide_query.reshape(tok_dev, -1, WIDE_HEAD_SIZE + ROPE)
    wide_plain = wide_heads_q[..., :WIDE_HEAD_SIZE]
    wide_turned = rotate(wide_heads_q[..., WIDE_HEAD_SIZE:].astype(jnp.float32), own_pos).astype(
        jnp.bfloat16
    )
    narrow_heads_q = narrow_query.reshape(tok_dev, -1, NARROW_HEAD_SIZE + ROPE)
    narrow_plain = narrow_heads_q[..., :NARROW_HEAD_SIZE]
    narrow_turned = rotate(
        narrow_heads_q[..., NARROW_HEAD_SIZE:].astype(jnp.float32), own_pos
    ).astype(jnp.bfloat16)
    wide_local = wide_plain.shape[1]
    narrow_local = narrow_plain.shape[1]
    wide_factor = (WIDE_HEAD_SIZE + ROPE) ** (-0.5)
    narrow_factor = (NARROW_HEAD_SIZE + ROPE) ** (-0.5)
    initial = empty_state(wide_local, tok_dev, WIDE_HEAD_SIZE) + empty_state(
        narrow_local, tok_dev, NARROW_HEAD_SIZE
    )
    pieces = (
        lax.all_gather(normed_latent, "sp", axis=0, tiled=True),
        lax.all_gather(turned_key, "sp", axis=0, tiled=True),
    )
    indices = jnp.arange(pieces[0].shape[0], dtype=jnp.int32)
    placing = lambda positions: positions
    latent_rows, turned_rows = pieces
    length_rows = latent_rows.shape[0]
    block = math.gcd(length_rows, 512)

    def one_block(block_index, inner):
        lat_block = lax.dynamic_slice_in_dim(latent_rows, block_index * block, block, 0)
        turned_block = lax.dynamic_slice_in_dim(turned_rows, block_index * block, block, 0)
        key_pos = placing(lax.dynamic_slice_in_dim(indices, block_index * block, block, 0))

        def work(current):
            visible = key_pos[None, :] <= own_pos[:, None]
            wide_keys = (
                jnp.dot(lat_block, wide_key_weight, preferred_element_type=jnp.float32)
                .astype(jnp.bfloat16)
                .reshape(block, wide_local, WIDE_HEAD_SIZE)
            )
            wide_values = (
                jnp.dot(lat_block, wide_value_weight, preferred_element_type=jnp.float32)
                .astype(jnp.bfloat16)
                .reshape(block, wide_local, WIDE_HEAD_SIZE)
            )
            narrow_keys = (
                jnp.dot(lat_block, narrow_key_weight, preferred_element_type=jnp.float32)
                .astype(jnp.bfloat16)
                .reshape(block, narrow_local, NARROW_HEAD_SIZE)
            )
            narrow_values = (
                jnp.dot(lat_block, narrow_value_weight, preferred_element_type=jnp.float32)
                .astype(jnp.bfloat16)
                .reshape(block, narrow_local, NARROW_HEAD_SIZE)
            )
            wide_state = update(
                current[:3],
                wide_plain,
                wide_turned,
                wide_keys,
                turned_block,
                wide_values,
                visible,
                wide_factor,
            )
            narrow_state = update(
                current[3:],
                narrow_plain,
                narrow_turned,
                narrow_keys,
                turned_block,
                narrow_values,
                visible,
                narrow_factor,
            )
            return wide_state + narrow_state

        return lax.cond(jnp.min(key_pos) <= last_pos, work, lambda current: current, inner)

    final = lax.fori_loop(0, length_rows // block, one_block, initial)
    wide_mix = finish(final[:3])
    narrow_mix = finish(final[3:])
    projected = lax.psum_scatter(
        (
            jnp.dot(wide_mix, out_wide, preferred_element_type=jnp.float32)
            + jnp.dot(narrow_mix, out_narrow, preferred_element_type=jnp.float32)
        ).astype(jnp.bfloat16),
        "tp",
        scatter_dimension=0,
        tiled=True,
    ).astype(jnp.float32)
    stream = (residual.astype(jnp.float32) + projected).astype(jnp.bfloat16)
    normed = rms_scale(stream.astype(jnp.float32), ffn_gain).astype(jnp.bfloat16)
    piece = lax.all_gather(normed, "tp", axis=0, tiled=True)
    gate_part = jnp.dot(piece, shared_gate, preferred_element_type=jnp.float32)
    up_part = jnp.dot(piece, shared_up, preferred_element_type=jnp.float32)
    active = (jax.nn.silu(gate_part) * up_part).astype(jnp.bfloat16)
    shared_terms = jnp.dot(active, shared_down, preferred_element_type=jnp.float32)
    shared = lax.psum_scatter(
        shared_terms.astype(jnp.bfloat16), "tp", scatter_dimension=0, tiled=True
    ).astype(jnp.float32)
    rows_here, top_count = routes.shape
    local_experts = expert_gate.shape[0]
    experts_all = local_experts * lax.axis_size(("sp", "tp"))
    capacity = max(2, 2 * top_count * rows_here // experts_all)
    model_width = normed.shape[1]
    flat_routes = routes.reshape(-1)
    assigned = flat_routes.shape[0]
    choose = (flat_routes[:, None] == jnp.arange(experts_all, dtype=jnp.int32)[None, :]).astype(
        jnp.float32
    )
    lower_mask = (jnp.arange(assigned)[:, None] > jnp.arange(assigned)[None, :]).astype(jnp.float32)
    earlier = jnp.dot(lower_mask, choose, precision=lax.Precision.HIGHEST)
    slots = jnp.sum(earlier * choose, axis=1).astype(jnp.int32)
    target = flat_routes * capacity + slots
    send_map = jnp.any(
        target.reshape(rows_here, top_count)[None, :, :]
        == jnp.arange(experts_all * capacity, dtype=jnp.int32)[:, None, None],
        axis=2,
    ).astype(jnp.bfloat16)
    outgoing = jnp.dot(send_map, normed, preferred_element_type=jnp.float32).astype(jnp.bfloat16)
    outgoing = outgoing.reshape(experts_all, capacity, model_width)
    incoming = lax.all_to_all(outgoing, ("sp", "tp"), split_axis=0, concat_axis=0, tiled=True)
    sources = incoming.shape[0] // local_experts
    grouped = incoming.reshape(sources, local_experts, incoming.shape[1], model_width)
    gate_part = jnp.einsum(
        "sxcd,xdf->sxcf", grouped, expert_gate, preferred_element_type=jnp.float32
    )
    up_part = jnp.einsum("sxcd,xdf->sxcf", grouped, expert_up, preferred_element_type=jnp.float32)
    active = (jax.nn.silu(gate_part) * up_part).astype(jnp.bfloat16)
    finished = jnp.einsum(
        "sxcf,xfd->sxcd", active, expert_down, preferred_element_type=jnp.float32
    ).astype(jnp.bfloat16)
    returned = lax.all_to_all(
        finished.reshape(incoming.shape), ("sp", "tp"), split_axis=0, concat_axis=0, tiled=True
    )
    picked = returned.reshape(experts_all * capacity, model_width)[target]
    routed = jnp.sum(
        picked.reshape(rows_here, top_count, model_width).astype(jnp.float32)
        * route_weights[:, :, None],
        axis=1,
    )
    return (stream.astype(jnp.float32) + shared + routed).astype(jnp.bfloat16)


def solution(mesh):
    placed = (
        P(("grp", "sp"), None),
        P(("grp", "sp"), None),
        P(("grp", "sp"), "tp"),
        P(("grp", "sp"), "tp"),
        P(None, "tp"),
        P(None, "tp"),
        P(None, "tp"),
        P(None, "tp"),
        P(),
        P("tp", None),
        P("tp", None),
        P(("grp", "sp", "tp"), None),
        P(),
        P(None, "tp"),
        P(None, "tp"),
        P("tp", None),
        P(("sp", "tp"), None, None),
        P(("sp", "tp"), None, None),
        P(("sp", "tp"), None, None),
        P(("grp", "sp", "tp"), None),
        P(("grp", "sp", "tp"), None),
    )
    return jax.shard_map(
        body, mesh=mesh, in_specs=placed, out_specs=P(("grp", "sp", "tp"), None), check_vma=False
    )
```

profile of v0, /device:TPU:11, one launch (start us, length us, event | category | flops | bytes accessed | tf_op | source)
XLA Modules:
  0.0 236.0 jit_solution(14494087974197204118)
XLA Ops:
  6.5 1.2 fusion.66
  7.8 1.8 fusion.68
  9.8 0.8 convert_element_type.143
  10.5 1.7 copy.48
  12.2 1.1 copy.47
  13.6 12.0 %all_gather.10 = bf16[1024,64]{0,1:T(8,128)(2,1)S(1)} all-gather(bf16[256,64]{0,1:T(8,128)(2,1)S(1)} %pad_maximum_fusion.2), channel_id=1, replica_groups=mesh['grp'=2,'sp'=4,'tp'=4] {'sp'}, dimensions={0}, use_global_device_ids=true | all-gather | bytes 163840 | tf_op jit(solution)/shard_map/all_gather | solution.py:118
  25.7 1.5 slice_convert_fusion
  27.9 11.8 %all-gather.3.cloned.1.call-done = bf16[1024,512]{1,0:T(8,128)(2,1)} async-done(((bf16[256,512]{1,0:T(8,128)(2,1)}), bf16[1024,512]{1,0:T(8,128)(2,1)}) %all-gather.3.cloned.1.call-update) | async-done | bytes 1048592 | tf_op jit(solution)/shard_map/all_gather | solution.py:117
  41.0 10.9 %while.24 = (s32[]{:T(128)}, f32[2,256]{1,0:T(2,128)S(1)}, f32[2,256]{1,0:T(2,128)S(1)}, f32[2,256,128]{2,1,0:T(8,128)S(1)}, f32[2,256]{1,0:T(2,128)S(1)}, /*ind...) while((s32[]{:T(128)}, f32[2,256]{1,0:T(2,128)S(1)}, ...), condition=%wide.region_9.10_spmd.clone, body=%wide.region_1.9_spmd.clone.sunk | while | flops 677055232 | bytes 22052092 | solution.py:177
  41.0 1.4 fusion.118
  43.5 5.8 %conditional.3 = ((f32[2,256]{1,0:T(2,128)S(1)}, f32[2,256]{1,0:T(2,128)S(1)}, f32[2,256,128]{2,1,0:T(8,128)S(1)}, f32[2,256]{1,0:T(2,128)S(1)}, f32[2,256]{1,0:T(2,128)}, /*index=5*/f32[2,256,64]{1,2,0:T(8,128)S(1)})) conditional(s32[]{:T(128)} %convert_element_type.241, (f32[2,256]{1,0:T(2,128)S(1)}, f32[2,256]{1,0:T(2,128)S(1)}, ...), branch_computations={%region_3.0_spmd, %region_4.8_spmd} | conditional | flops 677054720 | bytes 22046484 | solution.py:175
  43.6 1.4 convolution_convert_fusion.1
  49.4 1.4 fusion.118
  52.8 1.9 fusion.90
  54.8 2.1 fusion.36
  58.3 34.6 %reduce-scatter.3.cloned.1.call-done = bf16[64,4096]{1,0:T(8,128)(2,1)} async-done(((bf16[256,4096]{1,0:T(8,128)(2,1)}), bf16[64,4096]{1,0:T(8,128)(2,1)}) %reduce-scatter.3.cloned.1.call-update) | async-done | bytes 524304 | tf_op jit(solution)/shard_map/reduce_scatter | solution.py:180
  92.9 1.3 fusion.61
  94.3 1.2 fusion.63
  95.5 2.1 convolution_convert_fusion.6
  97.6 6.5 %all-to-all-start = ((bf16[16,16,4096]{2,1,0:T(8,128)(2,1)}), bf16[16,16,4096]{2,1,0:T(8,128)(2,1)}, u32[]{:S(2)}, u32[]{:S(2)}) async-start(bf16[16,16,4096]{2,1,0:T(8,128)(2,1)} %bitcast.126), calls=%async_computation.2 | async-start | bytes 4194304 | tf_op jit(solution)/shard_map/all_to_all | solution.py:220
  104.8 29.8 %all-gather.5.cloned.1.call-done = bf16[256,4096]{1,0:T(8,128)(2,1)} async-done(((bf16[64,4096]{1,0:T(8,128)(2,1)}), bf16[256,4096]{1,0:T(8,128)(2,1)}) %all-gather.5.cloned.1.call-update) | async-done | bytes 2097168 | tf_op jit(solution)/shard_map/all_gather | solution.py:191
  134.6 2.5 %fusion.91 = f32[256,128]{1,0:T(8,128)S(1)} fusion(bf16[256,4096]{1,0:T(8,128)(2,1)} %all-gather.5.cloned.1.call-done, bf16[4096,128]{1,0:T(8,128)(2,1)} %param.38), kind=kOutput, calls=%fused_computation.134 | convolution fusion | flops 268435456 | bytes 3276800 | tf_op jit(solution)/shard_map/dot_general | solution.py:192
  137.2 14.5 %all-to-all-done = bf16[16,16,4096]{2,1,0:T(8,128)(2,1)} async-done(((bf16[16,16,4096]{2,1,0:T(8,128)(2,1)}), bf16[16,16,4096]{2,1,0:T(8,128)(2,1)}, u32[]{:S(2)}, u32[]{:S(2)}) %all-to-all-start) | async-done | bytes 2097184 | tf_op jit(solution)/shard_map/all_to_all | solution.py:220
  151.7 2.8 %fusion.42 = f32[16,1,16,192]{3,2,0,1:T(8,128)S(1)} fusion(bf16[16,16,4096]{2,1,0:T(8,128)(2,1)} %all-to-all-done, bf16[1,4096,192]{1,2,0:T(8,128)(2,1)} %param.41), kind=kOutput, calls=%fused_computation.66 | convolution fusion | flops 402653184 | bytes 3866624 | tf_op jit(solution)/shard_map/sxcd,xdf->sxcf/dot_general | solution.py:223
  154.4 6.2 %convolution_convert_fusion.5 = bf16[16,16,4096]{2,1,0:T(8,128)(2,1)} fusion(bf16[1,192,4096]{2,1,0:T(8,128)(2,1)} %param.43, bf16[16,16,4096]{2,1,0:T(8,128)(2,1)} %all-to-all-done, bf16[1,4096,192]{1,2,0:T(8,128)(2,1)} %param.42, f32[16,1,16,192]{3,2,0,1:T(8,128)S(1)} %fusion.42), kind=kOutput, calls=%fused_computation.55 | convolution fusion | flops 806649856 | bytes 7536640 | tf_op jit(solution)/shard_map/sxcf,xfd->sxcd/dot_general | solution.py:228
  160.7 4.8 %all-to-all-start.1 = ((bf16[16,16,4096]{2,1,0:T(8,128)(2,1)}), bf16[16,16,4096]{2,1,0:T(8,128)(2,1)}, u32[]{:S(2)}, u32[]{:S(2)}) async-start(bf16[16,16,4096]{2,1,0:T(8,128)(2,1)} %convolution_convert_fusion.5), calls=%async_computation.3 | async-start | bytes 4194304 | tf_op jit(solution)/shard_map/all_to_all | solution.py:231
  165.7 4.8 %convolution_convert_fusion.4 = bf16[256,4096]{1,0:T(8,128)(2,1)} fusion(bf16[128,4096]{1,0:T(8,128)(2,1)} %param.40, bf16[256,4096]{1,0:T(8,128)(2,1)} %all-gather.5.cloned.1.call-done, bf16[4096,128]{1,0:T(8,128)(2,1)} %param.39, f32[256,128]{1,0:T(8,128)S(1)} %fusion.91), kind=kOutput, calls=%fused_computation.53 | convolution fusion | flops 538116096 | bytes 6422528 | tf_op jit(solution)/shard_map/dot_general | solution.py:195
  171.3 41.7 %all-to-all-done.1 = bf16[16,16,4096]{2,1,0:T(8,128)(2,1)} async-done(((bf16[16,16,4096]{2,1,0:T(8,128)(2,1)}), bf16[16,16,4096]{2,1,0:T(8,128)(2,1)}, u32[]{:S(2)}, u32[]{:S(2)}) %all-to-all-start.1) | async-done | bytes 2097184 | tf_op jit(solution)/shard_map/all_to_all | solution.py:231
  213.0 5.0 %gather_fusion = bf16[128,4096]{1,0:T(8,128)(2,1)} fusion(bf16[256,4096]{1,0:T(8,128)(2,1)} %bitcast.31, s32[1024]{0:T(1024)S(1)} %pad_clamp_fusion), kind=kCustom, calls=%fused_computation | custom fusion | bytes 2097664 | tf_op jit(solution)/shard_map/gather | solution.py:234
  218.1 3.4 %reshape.229 = f32[64,2,4096]{2,1,0:T(2,128)} reshape(bf16[128,4096]{1,0:T(8,128)(2,1)} %gather_fusion) | data formatting | bytes 3145728 | tf_op jit(solution)/shard_map/convert_element_type | solution.py:236
  221.4 5.7 %multiply_reduce_fusion = f32[64,4096]{1,0:T(8,128)} fusion(f32[64,2,4096]{2,1,0:T(2,128)} %reshape.229, f32[64,2]{1,0:T(8,128)S(1)} %copy.54), kind=kLoop, calls=%fused_computation.57 | loop fusion | flops 786432 | bytes 3146240 | tf_op jit(solution)/shard_map/reduce_sum | solution.py:235
  227.1 2.4 %fusion.65 = bf16[64,4096]{1,0:T(8,128)(2,1)} fusion(f32[64,4096]{1,0:T(8,128)} %multiply_reduce_fusion, bf16[64,4096]{1,0:T(8,128)(2,1)} %reduce-scatter.5.cloned.1.call-done, bf16[64,4096]{1,0:T(8,128)(2,1)S(1)} %copy-done.6, bf16[64,4096]{1,0:T(8,128)(2,1)S(1)} %copy-done.5), kind=kLoop, calls=%fused_computation.79 | loop fusion | flops 2359296 | bytes 3145728 | tf_op jit(solution)/shard_map/convert_element_type | solution.py:240
  (98 shorter events, 11.6 us)
Async XLA Ops:
  6.5 48.2 %copy-start = (bf16[256,4096]{1,0:T(8,128)(2,1)S(1)}, bf16[256,4096]{1,0:T(8,128)(2,1)}, u32[]{:S(2)}) copy-start(bf16[256,4096]{1,0:T(8,128)(2,1)} %param.34) | copy-start | bytes 6291460
  6.5 33.2 %all-gather.3.cloned.1.call-start = ((), (), s32[]{:S(2)}) async-start(), calls=%async_computation.4 | async-start | bytes 1310720 | tf_op jit(solution)/shard_map/all_gather | solution.py:117
  7.8 33.2 %copy-start.2 = (bf16[512,256]{1,0:T(8,128)(2,1)S(1)}, bf16[512,256]{1,0:T(8,128)(2,1)}, u32[]{:S(2)}) copy-start(bf16[512,256]{1,0:T(8,128)(2,1)} %param.29) | copy-start | bytes 786436
  7.8 33.2 %copy-start.3 = (bf16[512,256]{1,0:T(8,128)(2,1)S(1)}, bf16[512,256]{1,0:T(8,128)(2,1)}, u32[]{:S(2)}) copy-start(bf16[512,256]{1,0:T(8,128)(2,1)} %param.30) | copy-start | bytes 786436
  7.8 33.2 %copy-start.7 = (bf16[512,128]{1,0:T(8,128)(2,1)S(1)}, bf16[512,128]{1,0:T(8,128)(2,1)}, u32[]{:S(2)}) copy-start(bf16[512,128]{1,0:T(8,128)(2,1)} %param.31) | copy-start | bytes 393220
  7.8 33.2 %copy-start.8 = (bf16[512,128]{1,0:T(8,128)(2,1)S(1)}, bf16[512,128]{1,0:T(8,128)(2,1)}, u32[]{:S(2)}) copy-start(bf16[512,128]{1,0:T(8,128)(2,1)} %param.32) | copy-start | bytes 393220
  9.7 83.2 %reduce-scatter.3.cloned.1.call-start = ((), (), s32[]{:S(2)}) async-start(), calls=%async_computation.5 | async-start | bytes 2621440 | tf_op jit(solution)/shard_map/reduce_scatter | solution.py:180
  43.6 1.8 copy-start.14
  43.6 2.0 copy-start.10
  45.0 1.2 copy-start.1
  45.0 1.5 copy-start.9
  45.5 1.4 copy-start.11
  46.9 0.8 copy-start.12
  47.7 1.5 copy-start.13
  56.9 0.7 copy-start.16
  56.9 36.0 %copy-start.5 = (bf16[64,4096]{1,0:T(8,128)(2,1)S(1)}, bf16[64,4096]{1,0:T(8,128)(2,1)}, u32[]{:S(2)}) copy-start(bf16[64,4096]{1,0:T(8,128)(2,1)} %param.36) | copy-start | bytes 1572868
  56.9 37.4 %copy-start.15 = (f32[4096]{0:T(1024)S(1)}, f32[4096]{0:T(1024)}, u32[]{:S(2)}) copy-start(f32[4096]{0:T(1024)} %param.37) | copy-start | bytes 49156
  95.5 2.1 copy-start.4
  97.6 54.1 %all-to-all-start = ((bf16[16,16,4096]{2,1,0:T(8,128)(2,1)}), bf16[16,16,4096]{2,1,0:T(8,128)(2,1)}, u32[]{:S(2)}, u32[]{:S(2)}) async-start(bf16[16,16,4096]{2,1,0:T(8,128)(2,1)} %bitcast.126), calls=%async_computation.2 | async-start | bytes 4194304 | tf_op jit(solution)/shard_map/all_to_all | solution.py:220
  104.1 30.5 %all-gather.5.cloned.1.call-start = ((), (), s32[]{:S(2)}) async-start(), calls=%async_computation.6 | async-start | bytes 2621440 | tf_op jit(solution)/shard_map/all_gather | solution.py:191
  160.7 52.3 %all-to-all-start.1 = ((bf16[16,16,4096]{2,1,0:T(8,128)(2,1)}), bf16[16,16,4096]{2,1,0:T(8,128)(2,1)}, u32[]{:S(2)}, u32[]{:S(2)}) async-start(bf16[16,16,4096]{2,1,0:T(8,128)(2,1)} %convolution_convert_fusion.5), calls=%async_computation.3 | async-start | bytes 4194304 | tf_op jit(solution)/shard_map/all_to_all | solution.py:231
  165.5 61.7 %reduce-scatter.5.cloned.1.call-start = ((), (), s32[]{:S(2)}) async-start(), calls=%async_computation.7 | async-start | bytes 2621440 | tf_op jit(solution)/shard_map/reduce_scatter | solution.py:196
  170.5 0.7 copy-start.17
  221.4 5.7 %copy-start.6 = (bf16[64,4096]{1,0:T(8,128)(2,1)S(1)}, bf16[64,4096]{1,0:T(8,128)(2,1)}, u32[]{:S(2)}) copy-start(bf16[64,4096]{1,0:T(8,128)(2,1)} %reduce-scatter.3.cloned.1.call-done) | copy-start | bytes 1572868
Sparse Core Ops, SparseCore 0:
  9.8 29.8 all-gather.2
  57.0 35.8 reduce-scatter.2
  106.5 28.1 all-gather.4
  170.7 36.8 reduce-scatter.4
where the time goes:
time: 237 us; the launch traced here: 236 us
  waiting for transfers between devices  133 us (56%)
  matrix products  27.3 us (12%)
  other arithmetic  21.2 us (9%)
  local copies, waits for them, and re-layouts  15.9 us (7%)
  between operations  13.4 us (6%)
  blocking collectives  12 us (5%)
  starting transfers between devices  11.6 us (5%)
    all_to_all x1, waiting for transfers between devices, body(): lax.all_to_all(finished.reshape(incoming.shape), ('sp', 'tp'), split_axis...  41.7 us
    reduce_scatter x1, waiting for transfers between devices, body(): lax.psum_scatter((jnp.dot(wide_mix, out_wide, preferred_element_type=jnp....  34.6 us
    all_gather x1, waiting for transfers between devices, body(): piece = lax.all_gather(normed, 'tp', axis=0, tiled=True)  29.8 us
    all_to_all x1, waiting for transfers between devices, body(): lax.all_to_all(outgoing, ('sp', 'tp'), split_axis=0, concat_axis=0, tiled...  14.5 us
    all_gather x1, blocking collectives, body(): lax.all_gather(turned_key, 'sp', axis=0, tiled=True)  12 us
    all_gather x1, waiting for transfers between devices, body(): lax.all_gather(normed_latent, 'sp', axis=0, tiled=True)  11.8 us
    all_to_all x1, starting transfers between devices, body(): lax.all_to_all(outgoing, ('sp', 'tp'), split_axis=0, concat_axis=0, tiled...  6.5 us
    dot_general x1, matrix products, body(): jnp.einsum('sxcf,xfd->sxcd', active, expert_down, preferred_element_type=...  6.24 us
  transfers between devices with their start and end apart: 6, of which 5 were waited for; matrix products, arithmetic and copies ran while one was open for 12% of the time, Pallas kernels for 0%

commit v1 on v0

--- a/solution.py
+++ b/solution.py
@@ -188,7 +188,12 @@
     ).astype(jnp.float32)
     stream = (residual.astype(jnp.float32) + projected).astype(jnp.bfloat16)
     normed = rms_scale(stream.astype(jnp.float32), ffn_gain).astype(jnp.bfloat16)
-    piece = lax.all_gather(normed, "tp", axis=0, tiled=True)
+    ring = [normed]
+    for hop in range(3):
+        ring.append(lax.ppermute(ring[-1], "tp", [(dev, (dev + 1) % 4) for dev in range(4)]))
+    piece = jnp.roll(
+        jnp.concatenate(ring[::-1], axis=0), (lax.axis_index("tp") + 1) * ring[0].shape[0], axis=0
+    )
     gate_part = jnp.dot(piece, shared_gate, preferred_element_type=jnp.float32)
     up_part = jnp.dot(piece, shared_up, preferred_element_type=jnp.float32)
     active = (jax.nn.silu(gate_part) * up_part).astype(jnp.bfloat16)

time: 237 us -> 256 us (1.080)
  local copies, waits for them, and re-layouts: 15.9 us -> 23.8 us
  waiting for transfers between devices: 133 us -> 140 us
  starting transfers between devices: 11.6 us -> 17.9 us
    all_gather x1 -> x0, waiting for transfers between devices: 29.8 us -> none  [body(): piece = lax.all_gather(normed, 'tp', axis=0, tiled=True)]
    all_to_all x1, waiting for transfers between devices: 14.5 us -> 38.2 us  [body(): lax.all_to_all(outgoing, ('sp', 'tp'), split_axis=0, concat_axis=0, tiled...]
    ppermute x0 -> x3, waiting for transfers between devices: none -> 12 us  [body(): lax.ppermute(ring[-1], 'tp', [(dev, (dev + 1) % 4) for dev in range(4)])]
    unnamed x27 -> x36, local copies, waits for them, and re-layouts: 4.24 us -> 12.1 us
    ppermute x0 -> x3, starting transfers between devices: none -> 7.03 us  [body(): lax.ppermute(ring[-1], 'tp', [(dev, (dev + 1) % 4) for dev in range(4)])]
  transfers between devices with their start and end apart: 6 -> 8, of which waited for: 5 -> 6; matrix products, arithmetic and copies ran while one was open for 12% -> 14% of each run, Pallas kernels for 0% -> 0%
where the time goes in v1:
time: 256 us; the launch traced here: 255 us
  waiting for transfers between devices  140 us (55%)
  matrix products  25.6 us (10%)
  local copies, waits for them, and re-layouts  23.8 us (9%)
  other arithmetic  21.2 us (8%)
  starting transfers between devices  17.9 us (7%)
  between operations  13.4 us (5%)
  blocking collectives  12 us (5%)
    all_to_all x1, waiting for transfers between devices, body(): lax.all_to_all(finished.reshape(incoming.shape), ('sp', 'tp'), split_axis...  41.7 us
    all_to_all x1, waiting for transfers between devices, body(): lax.all_to_all(outgoing, ('sp', 'tp'), split_axis=0, concat_axis=0, tiled...  38.2 us
    reduce_scatter x1, waiting for transfers between devices, body(): lax.psum_scatter((jnp.dot(wide_mix, out_wide, preferred_element_type=jnp....  36 us
    unnamed x36, local copies, waits for them, and re-layouts  12.1 us
    all_gather x1, blocking collectives, body(): lax.all_gather(turned_key, 'sp', axis=0, tiled=True)  12 us
    ppermute x3, waiting for transfers between devices, body(): lax.ppermute(ring[-1], 'tp', [(dev, (dev + 1) % 4) for dev in range(4)])  12 us
    all_gather x1, waiting for transfers between devices, body(): lax.all_gather(normed_latent, 'sp', axis=0, tiled=True)  11.8 us
    ppermute x3, starting transfers between devices, body(): lax.ppermute(ring[-1], 'tp', [(dev, (dev + 1) % 4) for dev in range(4)])  7.03 us
  transfers between devices with their start and end apart: 8, of which 6 were waited for; matrix products, arithmetic and copies ran while one was open for 14% of the time, Pallas kernels for 0%

profile of v1, /device:TPU:11, one launch (start us, length us, event | category | flops | bytes accessed | tf_op | source)
XLA Modules:
  0.0 255.2 jit_solution(12644368900713638832)
XLA Ops:
  7.8 1.8 fusion.71
  10.5 1.7 copy.48
  13.6 12.0 %all_gather.7 = bf16[1024,64]{0,1:T(8,128)(2,1)S(1)} all-gather(bf16[256,64]{0,1:T(8,128)(2,1)S(1)} %pad_maximum_fusion.2), channel_id=1, replica_groups=mesh['grp'=2,'sp'=4,'tp'=4] {'sp'}, dimensions={0}, use_global_device_ids=true | all-gather | bytes 163840 | tf_op jit(solution)/shard_map/all_gather | solution.py:118
  25.7 1.5 slice_convert_fusion
  27.9 11.8 %all-gather.2.cloned.1.call-done = bf16[1024,512]{1,0:T(8,128)(2,1)} async-done(((bf16[256,512]{1,0:T(8,128)(2,1)}), bf16[1024,512]{1,0:T(8,128)(2,1)}) %all-gather.2.cloned.1.call-update) | async-done | bytes 1048592 | tf_op jit(solution)/shard_map/all_gather | solution.py:117
  41.0 11.1 %while.24 = (s32[]{:T(128)}, f32[2,256]{1,0:T(2,128)S(1)}, f32[2,256]{1,0:T(2,128)S(1)}, f32[2,256,128]{2,1,0:T(8,128)S(1)}, f32[2,256]{1,0:T(2,128)S(1)}, /*ind...) while((s32[]{:T(128)}, f32[2,256]{1,0:T(2,128)S(1)}, ...), condition=%wide.region_9.10_spmd.clone, body=%wide.region_1.9_spmd.clone.sunk | while | flops 677055232 | bytes 22052092 | solution.py:177
  41.0 1.4 fusion.120
  43.6 5.8 %conditional.3 = ((f32[2,256]{1,0:T(2,128)S(1)}, f32[2,256]{1,0:T(2,128)S(1)}, f32[2,256,128]{2,1,0:T(8,128)S(1)}, f32[2,256]{1,0:T(2,128)S(1)}, f32[2,256]{1,0:T(2,128)}, /*index=5*/f32[2,256,64]{1,2,0:T(8,128)S(1)})) conditional(s32[]{:T(128)} %convert_element_type.240, (f32[2,256]{1,0:T(2,128)S(1)}, f32[2,256]{1,0:T(2,128)S(1)}, ...), branch_computations={%region_3.0_spmd, %region_4.8_spmd} | conditional | flops 677054720 | bytes 22046484 | solution.py:175
  43.7 1.4 convolution_convert_fusion.1
  49.4 1.4 fusion.120
  52.9 1.9 fusion.95
  54.9 2.1 fusion.36
  57.1 36.0 %reduce-scatter.3.cloned.1.call-done = bf16[64,4096]{1,0:T(8,128)(2,1)} async-done(((bf16[256,4096]{1,0:T(8,128)(2,1)}), bf16[64,4096]{1,0:T(8,128)(2,1)}) %reduce-scatter.3.cloned.1.call-update) | async-done | bytes 524304 | tf_op jit(solution)/shard_map/reduce_scatter | solution.py:180
  93.0 1.3 fusion.64
  95.6 2.0 collective-permute-start
  97.6 6.1 %collective-permute-done = bf16[64,4096]{1,0:T(8,128)(2,1)} collective-permute-done((bf16[64,4096]{1,0:T(8,128)(2,1)S(1)}, bf16[64,4096]{1,0:T(8,128)(2,1)}, u32[]{:S(2)}, u32[]{:S(2)}) %collective-permute-start) | collective-permute-done | bytes 524320 | tf_op jit(solution)/shard_map/ppermute | solution.py:193
  103.7 2.6 %collective-permute-start.1 = (bf16[64,4096]{1,0:T(8,128)(2,1)}, bf16[64,4096]{1,0:T(8,128)(2,1)}, u32[]{:S(2)}, u32[]{:S(2)}) collective-permute-start(bf16[64,4096]{1,0:T(8,128)(2,1)} %collective-permute-done), channel_id=1, source_target_pairs={{0,1},{1,2},{2,3},{3,0},{4,5},{5,6},{6,7},{7,4},{8,9},{9,10},{10,1... | collective-permute-start | bytes 1572872 | tf_op jit(solution)/shard_map/ppermute | solution.py:193
  106.9 5.9 %collective-permute-done.1 = bf16[64,4096]{1,0:T(8,128)(2,1)} collective-permute-done((bf16[64,4096]{1,0:T(8,128)(2,1)}, bf16[64,4096]{1,0:T(8,128)(2,1)}, u32[]{:S(2)}, u32[]{:S(2)}) %collective-permute-start.1) | collective-permute-done | bytes 524320 | tf_op jit(solution)/shard_map/ppermute | solution.py:193
  112.8 2.5 collective-permute-start.2
  115.4 2.1 convolution_convert_fusion.6
  117.5 5.8 %all-to-all-start = ((bf16[16,16,4096]{2,1,0:T(8,128)(2,1)}), bf16[16,16,4096]{2,1,0:T(8,128)(2,1)}, u32[]{:S(2)}, u32[]{:S(2)}) async-start(bf16[16,16,4096]{2,1,0:T(8,128)(2,1)} %bitcast.124), calls=%async_computation.2 | async-start | bytes 4194304 | tf_op jit(solution)/shard_map/all_to_all | solution.py:225
  130.0 1.9 copy-done.4
  132.6 38.2 %all-to-all-done = bf16[16,16,4096]{2,1,0:T(8,128)(2,1)} async-done(((bf16[16,16,4096]{2,1,0:T(8,128)(2,1)}), bf16[16,16,4096]{2,1,0:T(8,128)(2,1)}, u32[]{:S(2)}, u32[]{:S(2)}) %all-to-all-start) | async-done | bytes 2097184 | tf_op jit(solution)/shard_map/all_to_all | solution.py:225
  170.8 2.8 %fusion.46 = f32[16,1,16,192]{3,2,0,1:T(8,128)S(1)} fusion(bf16[16,16,4096]{2,1,0:T(8,128)(2,1)} %all-to-all-done, bf16[1,4096,192]{1,2,0:T(8,128)(2,1)} %param.41), kind=kOutput, calls=%fused_computation.70 | convolution fusion | flops 402653184 | bytes 3866624 | tf_op jit(solution)/shard_map/sxcd,xdf->sxcf/dot_general | solution.py:228
  173.6 6.3 %convolution_convert_fusion.5 = bf16[16,16,4096]{2,1,0:T(8,128)(2,1)} fusion(bf16[1,192,4096]{2,1,0:T(8,128)(2,1)} %param.43, bf16[16,16,4096]{2,1,0:T(8,128)(2,1)} %all-to-all-done, bf16[1,4096,192]{1,2,0:T(8,128)(2,1)} %param.42, f32[16,1,16,192]{3,2,0,1:T(8,128)S(1)} %fusion.46), kind=kOutput, calls=%fused_computation.55 | convolution fusion | flops 806649856 | bytes 7536640 | tf_op jit(solution)/shard_map/sxcf,xfd->sxcd/dot_general | solution.py:233
  179.9 4.8 %all-to-all-start.1 = ((bf16[16,16,4096]{2,1,0:T(8,128)(2,1)}), bf16[16,16,4096]{2,1,0:T(8,128)(2,1)}, u32[]{:S(2)}, u32[]{:S(2)}) async-start(bf16[16,16,4096]{2,1,0:T(8,128)(2,1)} %convolution_convert_fusion.5), calls=%async_computation.3 | async-start | bytes 4194304 | tf_op jit(solution)/shard_map/all_to_all | solution.py:236
  184.9 4.8 %convolution_convert_fusion.4 = bf16[256,4096]{1,0:T(8,128)(2,1)} fusion(bf16[128,4096]{1,0:T(8,128)(2,1)} %param.40, f32[256,128]{1,0:T(8,128)S(1)} %fusion.37, bf16[4096,128]{1,0:T(8,128)(2,1)} %param.38, bf16[512,4096]{1,0:T(8,128)(2,1)} %copy-done.4, s32[]{:T(128)S(6)} %select_n.54), kind=kOutput, calls=%fused_computation.53 | convolution fusion | flops 538116096 | bytes 6422532 | tf_op jit(solution)/shard_map/dot_general | solution.py:200
  190.5 41.7 %all-to-all-done.1 = bf16[16,16,4096]{2,1,0:T(8,128)(2,1)} async-done(((bf16[16,16,4096]{2,1,0:T(8,128)(2,1)}), bf16[16,16,4096]{2,1,0:T(8,128)(2,1)}, u32[]{:S(2)}, u32[]{:S(2)}) %all-to-all-start.1) | async-done | bytes 2097184 | tf_op jit(solution)/shard_map/all_to_all | solution.py:236
  232.2 5.0 %gather_fusion = bf16[128,4096]{1,0:T(8,128)(2,1)} fusion(bf16[256,4096]{1,0:T(8,128)(2,1)} %bitcast.31, s32[1024]{0:T(1024)S(1)} %pad_clamp_fusion), kind=kCustom, calls=%fused_computation | custom fusion | bytes 2097664 | tf_op jit(solution)/shard_map/gather | solution.py:239
  237.2 3.4 %reshape.229 = f32[64,2,4096]{2,1,0:T(2,128)} reshape(bf16[128,4096]{1,0:T(8,128)(2,1)} %gather_fusion) | data formatting | bytes 3145728 | tf_op jit(solution)/shard_map/convert_element_type | solution.py:241
  240.6 5.7 %multiply_reduce_fusion = f32[64,4096]{1,0:T(8,128)} fusion(f32[64,2,4096]{2,1,0:T(2,128)} %reshape.229, f32[64,2]{1,0:T(8,128)S(1)} %copy.54), kind=kLoop, calls=%fused_computation.57 | loop fusion | flops 786432 | bytes 3146240 | tf_op jit(solution)/shard_map/reduce_sum | solution.py:240
  246.3 2.4 fusion.68
  (111 shorter events, 21.9 us)
Async XLA Ops:
  6.5 48.4 %copy-start = (bf16[256,4096]{1,0:T(8,128)(2,1)S(1)}, bf16[256,4096]{1,0:T(8,128)(2,1)}, u32[]{:S(2)}) copy-start(bf16[256,4096]{1,0:T(8,128)(2,1)} %param.34) | copy-start | bytes 6291460
  6.5 33.2 %all-gather.2.cloned.1.call-start = ((), (), s32[]{:S(2)}) async-start(), calls=%async_computation.4 | async-start | bytes 1310720 | tf_op jit(solution)/shard_map/all_gather | solution.py:117
  7.8 33.2 %copy-start.2 = (bf16[512,256]{1,0:T(8,128)(2,1)S(1)}, bf16[512,256]{1,0:T(8,128)(2,1)}, u32[]{:S(2)}) copy-start(bf16[512,256]{1,0:T(8,128)(2,1)} %param.29) | copy-start | bytes 786436
  7.8 33.2 %copy-start.3 = (bf16[512,256]{1,0:T(8,128)(2,1)S(1)}, bf16[512,256]{1,0:T(8,128)(2,1)}, u32[]{:S(2)}) copy-start(bf16[512,256]{1,0:T(8,128)(2,1)} %param.30) | copy-start | bytes 786436
  7.8 33.2 %copy-start.7 = (bf16[512,128]{1,0:T(8,128)(2,1)S(1)}, bf16[512,128]{1,0:T(8,128)(2,1)}, u32[]{:S(2)}) copy-start(bf16[512,128]{1,0:T(8,128)(2,1)} %param.31) | copy-start | bytes 393220
  7.8 33.2 %copy-start.8 = (bf16[512,128]{1,0:T(8,128)(2,1)S(1)}, bf16[512,128]{1,0:T(8,128)(2,1)}, u32[]{:S(2)}) copy-start(bf16[512,128]{1,0:T(8,128)(2,1)} %param.32) | copy-start | bytes 393220
  9.7 83.3 %reduce-scatter.3.cloned.1.call-start = ((), (), s32[]{:S(2)}) async-start(), calls=%async_computation.5 | async-start | bytes 2621440 | tf_op jit(solution)/shard_map/reduce_scatter | solution.py:180
  43.6 1.8 copy-start.15
  43.6 2.0 copy-start.10
  45.1 1.2 copy-start.1
  45.1 1.5 copy-start.9
  45.6 1.3 copy-start.11
  47.0 0.8 copy-start.13
  47.8 1.5 copy-start.14
  57.0 36.0 %copy-start.5 = (bf16[64,4096]{1,0:T(8,128)(2,1)S(1)}, bf16[64,4096]{1,0:T(8,128)(2,1)}, u32[]{:S(2)}) copy-start(bf16[64,4096]{1,0:T(8,128)(2,1)} %param.36) | copy-start | bytes 1572868
  57.0 37.3 %copy-start.16 = (f32[4096]{0:T(1024)S(1)}, f32[4096]{0:T(1024)}, u32[]{:S(2)}) copy-start(f32[4096]{0:T(1024)} %param.37) | copy-start | bytes 49156
  57.0 49.3 %copy-start.17 = (s32[64,2]{0,1:T(2,128)S(1)}, s32[64,2]{0,1:T(2,128)}, u32[]{:S(2)}) copy-start(s32[64,2]{0,1:T(2,128)} %param.44) | copy-start | bytes 1540
  95.6 8.1 %collective-permute-start = (bf16[64,4096]{1,0:T(8,128)(2,1)S(1)}, bf16[64,4096]{1,0:T(8,128)(2,1)}, u32[]{:S(2)}, u32[]{:S(2)}) collective-permute-start(bf16[64,4096]{1,0:T(8,128)(2,1)S(1)} %fusion.66), channel_id=1, source_target_pairs={{0,1},{1,2},{2,3},{3,0},{4,5},{5,6},{6,7},{7,4},{8,9},{9,10},{10,1... | collective-permute-start | bytes 1572872 | tf_op jit(solution)/shard_map/ppermute | solution.py:193
  103.7 9.0 %collective-permute-start.1 = (bf16[64,4096]{1,0:T(8,128)(2,1)}, bf16[64,4096]{1,0:T(8,128)(2,1)}, u32[]{:S(2)}, u32[]{:S(2)}) collective-permute-start(bf16[64,4096]{1,0:T(8,128)(2,1)} %collective-permute-done), channel_id=1, source_target_pairs={{0,1},{1,2},{2,3},{3,0},{4,5},{5,6},{6,7},{7,4},{8,9},{9,10},{10,1... | collective-permute-start | bytes 1572872 | tf_op jit(solution)/shard_map/ppermute | solution.py:193
  112.8 10.6 %collective-permute-start.2 = (bf16[64,4096]{1,0:T(8,128)(2,1)}, bf16[64,4096]{1,0:T(8,128)(2,1)}, u32[]{:S(2)}, u32[]{:S(2)}) collective-permute-start(bf16[64,4096]{1,0:T(8,128)(2,1)} %collective-permute-done.1), channel_id=1, source_target_pairs={{0,1},{1,2},{2,3},{3,0},{4,5},{5,6},{6,7},{7,4},{8,9},{9,10},{10,1... | collective-permute-start | bytes 1572872 | tf_op jit(solution)/shard_map/ppermute | solution.py:193
  117.5 53.3 %all-to-all-start = ((bf16[16,16,4096]{2,1,0:T(8,128)(2,1)}), bf16[16,16,4096]{2,1,0:T(8,128)(2,1)}, u32[]{:S(2)}, u32[]{:S(2)}) async-start(bf16[16,16,4096]{2,1,0:T(8,128)(2,1)} %bitcast.124), calls=%async_computation.2 | async-start | bytes 4194304 | tf_op jit(solution)/shard_map/all_to_all | solution.py:225
  126.6 5.3 %copy-start.12 = (bf16[4096,128]{1,0:T(8,128)(2,1)S(1)}, bf16[4096,128]{1,0:T(8,128)(2,1)}, u32[]{:S(2)}) copy-start(bf16[4096,128]{1,0:T(8,128)(2,1)} %param.39) | copy-start | bytes 3145732
  130.0 1.9 copy-start.4
  179.9 52.3 %all-to-all-start.1 = ((bf16[16,16,4096]{2,1,0:T(8,128)(2,1)}), bf16[16,16,4096]{2,1,0:T(8,128)(2,1)}, u32[]{:S(2)}, u32[]{:S(2)}) async-start(bf16[16,16,4096]{2,1,0:T(8,128)(2,1)} %convolution_convert_fusion.5), calls=%async_computation.3 | async-start | bytes 4194304 | tf_op jit(solution)/shard_map/all_to_all | solution.py:236
  184.6 61.7 %reduce-scatter.5.cloned.1.call-start = ((), (), s32[]{:S(2)}) async-start(), calls=%async_computation.6 | async-start | bytes 2621440 | tf_op jit(solution)/shard_map/reduce_scatter | solution.py:201
  189.7 0.7 copy-start.18
  240.6 5.7 %copy-start.6 = (bf16[64,4096]{1,0:T(8,128)(2,1)S(1)}, bf16[64,4096]{1,0:T(8,128)(2,1)}, u32[]{:S(2)}) copy-start(bf16[64,4096]{1,0:T(8,128)(2,1)} %reduce-scatter.3.cloned.1.call-done) | copy-start | bytes 1572868
Sparse Core Ops, SparseCore 0:
  9.8 29.8 all-gather.1
  57.2 35.8 reduce-scatter.2
  189.9 36.7 reduce-scatter.4
